TPU v7x, 32 devices: a whole 2x2x4 slice. The times are simulated.
32 devices in a mesh: dp: 4 (over y, x), kv: 4 (over z), tp: 2 (over core).
Axes of the slice: x: 2, y: 2, z: 4, core: 2. Of those that a mesh axis runs over, the one named last changes fastest.
Arguments:
- tokens: bfloat16 [16, 16, 2048], P('dp', None, 'kv'), may hold values from -6 to 6
- norm_gain: float32 [2048], P('kv'), may hold values from 0.1 to 1.9
- w_query: bfloat16 [2048, 1024], P('kv', 'tp'), may hold values from -0.125 to 0.125
- w_key: bfloat16 [2048, 1024], P('kv', 'tp'), may hold values from -0.125 to 0.125
- w_value: bfloat16 [2048, 1024], P('kv', 'tp'), may hold values from -0.125 to 0.125
- w_forget: bfloat16 [2048, 16], replicated, may hold values from -0.125 to 0.125
- forget_bias: float32 [16], replicated, may hold values from -2 to 4
- query_gain: float32 [64], replicated, may hold values from 0.1 to 1.9
- key_gain: float32 [64], replicated, may hold values from 0.1 to 1.9
- head_gain: float32 [64], replicated, may hold values from 0.1 to 1.9
- w_out: bfloat16 [1024, 2048], P('tp', 'kv'), may hold values from -0.1875 to 0.1875
- key_cache: bfloat16 [16, 2048, 1024], P('dp', 'kv', 'tp'), may hold values from -240 to 240
- value_cache: bfloat16 [16, 2048, 1024], P('dp', 'kv', 'tp'), may hold values from -6 to 6
- gate_cache: float32 [16, 16, 2048], P('dp', 'tp', 'kv'), may hold values from -242 to 0, as said below
- lengths: int32 [16], P('dp'), may hold values from 1005 to 2028
- accepted: int32 [16], P('dp'), may hold values from 0 to 4
- parents: int32 [16, 16], P('dp'), may hold values from -1 to 14, as said below
Outputs:
- layer_out: bfloat16 [16, 16, 2048], P('dp', None, 'kv')
- new_keys: bfloat16 [16, 2048, 1024], P('dp', 'kv', 'tp')
- new_values: bfloat16 [16, 2048, 1024], P('dp', 'kv', 'tp')
- proposal_gates: float32 [16, 16, 16], P('dp', None, 'tp')
Inputs may be any that keep to these rules, and one draw needn't show every extreme that they name: `gate_cache`: each entry is the running sum of log forget gates up to its position, so entries never rise along positions; entries at and after lengths hold the last step's proposals in order. `parents`: proposal 0 follows the last accepted token (parent -1); every other proposal's parent is one of the three proposals before it.
All inputs are finite; a program needn't handle non-finite values.
Results may differ from a plain program's by a relative error of at most 0.0051.
The roundings to bfloat16 on the way count: a program that leaves them out, or rounds other values in their place, can miss the bound.
Values may be sent and summed in bfloat16 or wider, within the bound.
A program may use at most 64 MiB of HBM per device.

v0:
```python
import jax
import jax.numpy as jnp
from jax import lax
from jax.sharding import PartitionSpec as P

EPSILON = 1e-06
MASKED = -1e30


def head_norm(head_rows, gain_vec):
    mean_square = jnp.mean(head_rows * head_rows, axis=-1, keepdims=True)
    return head_rows * lax.rsqrt(mean_square + EPSILON) * gain_vec


def ancestry(parents):
    count_all = parents.shape[1]
    step_ids = jnp.arange(count_all, dtype=jnp.int32)
    step_matrix = (parents[:, :, None] == step_ids[None, None, :]).astype(jnp.float32)
    identity = jnp.broadcast_to(jnp.eye(count_all, dtype=jnp.float32), step_matrix.shape)

    def extend(turn_index, ancestors):
        return identity + jnp.einsum(
            "sij,sjk->sik", step_matrix, ancestors, precision=lax.Precision.HIGHEST
        )

    return lax.fori_loop(0, count_all, extend, identity)


def combine(earlier, later):
    earlier_max, earlier_total, earlier_sum = earlier
    later_max, later_total, later_sum = later
    row_max = jnp.maximum(earlier_max, later_max)
    earlier_scale = jnp.exp(earlier_max - row_max)
    later_scale = jnp.exp(later_max - row_max)
    spread = earlier_max.shape + (-1,)
    joined = (
        earlier_sum.reshape(spread) * earlier_scale[..., None]
        + later_sum.reshape(spread) * later_scale[..., None]
    )
    return (
        row_max,
        earlier_total * earlier_scale + later_total * later_scale,
        joined.reshape(earlier_sum.shape),
    )


def block_part(scores, live_mask, block_values):
    seq_count, heads_local, prop_count, key_count = scores.shape
    row_max = jnp.max(scores, axis=3)
    weights = jnp.where(live_mask, jnp.exp(scores - row_max[..., None]), 0.0)
    row_total = jnp.sum(weights, axis=3)
    weighted = jnp.einsum(
        "shpk,skhd->sphd",
        weights.astype(jnp.bfloat16),
        block_values,
        preferred_element_type=jnp.float32,
    )
    return (
        jnp.transpose(row_max, (0, 2, 1)),
        jnp.transpose(row_total, (0, 2, 1)),
        weighted.reshape(seq_count, prop_count, -1),
    )


def finish_rows(row_sums, inverse, query_gain, key_gain, heads_local):
    head_width = row_sums.shape[1] // 3
    head_size = head_width // heads_local
    row_count = row_sums.shape[0]
    raw_sums = row_sums * inverse[:, None]
    queries = head_norm(
        raw_sums[:, :head_width].reshape(row_count, heads_local, head_size), query_gain
    )
    keyed = head_norm(
        raw_sums[:, head_width : 2 * head_width].reshape(row_count, heads_local, head_size),
        key_gain,
    )
    return jnp.concatenate(
        [
            queries.reshape(row_count, head_width),
            keyed.reshape(row_count, head_width),
            raw_sums[:, 2 * head_width :],
        ],
        axis=1,
    ).astype(jnp.bfloat16)


def flatten_part(part_triple, rows_all):
    part_max, part_total, part_sum = part_triple
    return (
        part_max.reshape(rows_all, -1),
        part_total.reshape(rows_all, -1),
        part_sum.reshape(rows_all, -1),
    )


def shards(
    tokens,
    norm_gain,
    w_query,
    w_key,
    w_value,
    w_forget,
    forget_bias,
    query_gain,
    key_gain,
    head_gain,
    w_out,
    key_cache,
    value_cache,
    gate_cache,
    lengths,
    accepted,
    parents,
):
    seq_count, prop_count, width_in = tokens.shape
    pos_dev = key_cache.shape[1]
    heads_local = gate_cache.shape[1]
    head_width = key_cache.shape[2]
    head_size = head_width // heads_local
    rows_all = seq_count * prop_count
    full_width = w_forget.shape[0]
    kv_index = lax.axis_index("kv")
    tp_index = lax.axis_index("tp")
    flattened = tokens.reshape(rows_all, width_in).astype(jnp.float32)
    squares = jnp.sum(flattened * flattened, axis=1)
    scaled = (flattened * norm_gain).astype(jnp.bfloat16)
    w_rows = lax.dynamic_slice_in_dim(w_forget, kv_index * width_in, width_in, 0)
    gate_part = jnp.dot(scaled, w_rows, preferred_element_type=jnp.float32)
    w_joined = jnp.concatenate([w_query, w_key, w_value], axis=1)
    summed, gate_sum, square_sum = lax.psum(
        (jnp.dot(scaled, w_joined, preferred_element_type=jnp.float32), gate_part, squares), "kv"
    )
    inverse = lax.rsqrt(square_sum / full_width + EPSILON)
    joined = finish_rows(summed, inverse, query_gain, key_gain, heads_local)
    log_all = jax.nn.log_sigmoid(gate_sum * inverse[:, None] + forget_bias)
    log_own = lax.dynamic_slice_in_dim(log_all, tp_index * heads_local, heads_local, 1)
    log_own = log_own.reshape(seq_count, prop_count, heads_local)
    queries = joined[:, :head_width].reshape(seq_count, prop_count, heads_local, head_size)
    keys_new = joined[:, head_width : 2 * head_width].reshape(
        seq_count, prop_count, heads_local, head_size
    )
    values_new = joined[:, 2 * head_width :].reshape(seq_count, prop_count, heads_local, head_size)
    ancestors = ancestry(parents)
    path_sum = jnp.einsum("sij,sjh->sih", ancestors, log_own, precision=lax.Precision.HIGHEST)
    base_pos = lengths + accepted
    positions = kv_index * pos_dev + jnp.arange(pos_dev, dtype=jnp.int32)
    score_scale = head_size ** (-0.5)
    cached_keys = key_cache.reshape(seq_count, pos_dev, heads_local, head_size)
    cached_values = value_cache.reshape(seq_count, pos_dev, heads_local, head_size)
    scores = jnp.einsum("sphd,skhd->shpk", queries, cached_keys, preferred_element_type=jnp.float32)
    scores = scores * score_scale - gate_cache[:, :, None, :]
    live_mask = (positions[None, :] < base_pos[:, None])[:, None, None, :]
    scores = jnp.where(live_mask, scores, MASKED)
    local_part = block_part(scores, live_mask, cached_values)
    hit_mask = positions[None, :] == (base_pos - 1)[:, None]
    boundary_local = jnp.sum(jnp.where(hit_mask[:, None, :], gate_cache, 0.0), axis=2)
    tree_live = (ancestors > 0.5)[:, None, :, :]
    boundary = lax.psum(boundary_local, "kv")
    flat_max, flat_total, flat_sum = flatten_part(local_part, rows_all)
    got_max, got_total, got_sum = (
        lax.all_to_all(flat_max[None], "kv", split_axis=1, concat_axis=0, tiled=True),
        lax.all_to_all(flat_total[None], "kv", split_axis=1, concat_axis=0, tiled=True),
        lax.all_to_all(flat_sum[None], "kv", split_axis=1, concat_axis=0, tiled=True),
    )
    top = jnp.max(got_max, axis=0)
    factors = jnp.exp(got_max - top[None])
    own_rows = got_max.shape[1]
    summed_rows = jnp.sum(
        got_sum.reshape(got_sum.shape[0], own_rows, heads_local, head_size) * factors[..., None],
        axis=0,
    )
    merged = (top, jnp.sum(got_total * factors, axis=0), summed_rows.reshape(own_rows, head_width))
    tree_scores = jnp.einsum(
        "sphd,sjhd->shpj", queries, keys_new, preferred_element_type=jnp.float32
    )
    tree_scores = (
        tree_scores * score_scale
        - jnp.transpose(path_sum, (0, 2, 1))[:, :, None, :]
        - boundary[:, :, None, None]
    )
    tree_scores = jnp.where(tree_live, tree_scores, MASKED)
    tree_max, tree_total, tree_sum = flatten_part(
        block_part(tree_scores, tree_live, values_new), rows_all
    )
    row_lower = kv_index * own_rows
    merged = combine(
        merged,
        (
            lax.dynamic_slice_in_dim(tree_max, row_lower, own_rows, 0),
            lax.dynamic_slice_in_dim(tree_total, row_lower, own_rows, 0),
            lax.dynamic_slice_in_dim(tree_sum, row_lower, own_rows, 0),
        ),
    )
    row_max, row_total, weighted = merged
    attended = weighted.reshape(own_rows, heads_local, head_size) / row_total[..., None]
    own_normed = head_norm(attended, head_gain).astype(jnp.bfloat16).reshape(own_rows, head_width)
    normed = lax.all_gather(own_normed, "kv", axis=0, tiled=True)
    out_term = jnp.dot(normed, w_out, preferred_element_type=jnp.float32)
    layer_out = lax.psum(out_term.astype(jnp.bfloat16), "tp")
    layer_out = layer_out.reshape(seq_count, prop_count, -1)
    new_rows = jnp.concatenate(
        [
            keys_new.reshape(seq_count, prop_count, head_width),
            values_new.reshape(seq_count, prop_count, head_width),
        ],
        axis=2,
    )
    slot_index = positions[None, :, None] - base_pos[:, None, None]
    placing = slot_index == jnp.arange(prop_count, dtype=jnp.int32)[None, None, :]
    written = jnp.einsum(
        "skp,spc->skc", placing.astype(jnp.bfloat16), new_rows, preferred_element_type=jnp.float32
    ).astype(jnp.bfloat16)
    hit_rows = jnp.any(placing, axis=2)[..., None]
    new_keys = jnp.where(hit_rows, written[..., :head_width], key_cache)
    new_values = jnp.where(hit_rows, written[..., head_width:], value_cache)
    return (layer_out, new_keys, new_values, log_own)


def solution(mesh):
    placed = (
        P("dp", None, "kv"),
        P("kv"),
        P("kv", "tp"),
        P("kv", "tp"),
        P("kv", "tp"),
        P(),
        P(),
        P(),
        P(),
        P(),
        P("tp", "kv"),
        P("dp", "kv", "tp"),
        P("dp", "kv", "tp"),
        P("dp", "tp", "kv"),
        P("dp"),
        P("dp"),
        P("dp", None),
    )
    return jax.shard_map(
        shards,
        mesh=mesh,
        in_specs=placed,
        out_specs=(
            P("dp", None, "kv"),
            P("dp", "kv", "tp"),
            P("dp", "kv", "tp"),
            P("dp", None, "tp"),
        ),
        check_vma=False,
    )
```

profile of v0, /device:TPU:0, one launch (start us, length us, event | category | flops | bytes accessed | tf_op | source)
XLA Modules:
  0.0 129.3 jit_solution(6320880123169172122)
XLA Ops:
  7.2 0.9 fusion.29
  8.3 2.6 %fusion.6 = f32[64,1536]{1,0:T(8,128)} fusion(bf16[64,512]{1,0:T(8,128)(2,1)S(1)} %fusion.29, bf16[512,512]{1,0:T(8,128)(2,1)} %param.23, bf16[512,512]{1,0:T(8,128)(2,1)} %param.22, bf16[512,512]{1,0:T(8,128)(2,1)} %param.21), kind=kOutput, calls=%fused_computation.9 | convolution fusion | flops 105381888 | bytes 2031616 | tf_op jit(solution)/shard_map/dot_general | solution.py:131
  11.2 4.2 %while.11 = (s32[]{:T(128)}, f32[4,16,16]{2,1,0:T(8,128)S(1)}, s32[4,16]{1,0:T(4,128)S(1)}, f32[16,16]{1,0:T(8,128)S(1)}, s32[]{:T(128)}) while((s32[]{:T(128)}, f32[4,16,16]{2,1,0:T(8,128)S(1)}, s32[4,16]{1,0:T(4,128)S(1)}, f32[16,16]{1,0:T(8,128)S(1)}, s32[]{:T(128)}) %tuple.50), condition=%wide.region_8.9_spmd.clone, body=%wide.region_7.8_spmd.clone.sunk | while | flops 199682 | bytes 17725 | solution.py:26
  11.3 0.2 convolution_add_fusion.2
  11.5 0.2 convolution_add_fusion.2
  11.8 0.2 convolution_add_fusion.2
  12.1 0.2 convolution_add_fusion.2
  12.3 0.2 convolution_add_fusion.2
  12.6 0.2 convolution_add_fusion.2
  12.8 0.2 convolution_add_fusion.2
  13.1 0.2 convolution_add_fusion.2
  13.4 0.2 convolution_add_fusion.2
  13.6 0.2 convolution_add_fusion.2
  13.9 0.2 convolution_add_fusion.2
  14.2 0.2 convolution_add_fusion.2
  14.4 0.2 convolution_add_fusion.2
  14.7 0.2 convolution_add_fusion.2
  15.0 0.2 convolution_add_fusion.2
  15.6 0.8 fusion.39
  16.4 20.4 %all-reduce = (f32[64]{0:T(128)S(1)}, f32[4,8]{1,0:T(4,128)S(1)}, f32[64,16]{0,1:T(8,128)S(1)}) all-reduce(f32[64]{0:T(128)S(1)} %reduce_sum.86, f32[4,8]{1,0:T(4,128)S(1)} %select_reduce_fusion, f32[64,16]{0,1:T(8,128)S(1)} %fusion.39), channel_id=1, replica_groups=mesh['dp'=4,'kv'=4,'tp'=2] {'kv'}, use_global_device_ids=true, to_apply=%region_2.0 | all-reduce | flops 1120 | bytes 8960 | tf_op jit(solution)/shard_map/psum | solution.py:130
  37.4 4.3 %copy.136 = bf16[4,512,512]{1,2,0:T(8,128)(2,1)} copy(bf16[4,512,512]{2,1,0:T(8,128)(2,1)} %param.30) | data formatting | bytes 4194304 | tf_op args[11]
  41.7 2.4 %copy.138 = bf16[4,512,512]{1,2,0:T(8,128)(2,1)} copy(bf16[4,512,512]{2,1,0:T(8,128)(2,1)S(1)} %copy-done.1) | data formatting | bytes 4194304 | tf_op args[12]
  44.3 6.7 %all-reduce.4.cloned.1.call-done = f32[64,1536]{1,0:T(8,128)} async-done(((f32[64,1536]{1,0:T(8,128)}), f32[64,1536]{1,0:T(8,128)}) %all-reduce.4.cloned.1.call-update) | async-done | bytes 393232 | tf_op jit(solution)/shard_map/psum | solution.py:130
  51.0 1.1 broadcast_multiply_fusion
  53.9 2.1 %fusion.57 = (f32[4,8,16]{2,1,0:T(8,128)S(1)}, f32[4,8,16,512]{3,2,1,0:T(8,128)S(1)}) fusion(f32[4,8,512]{2,1,0:T(8,128)S(1)} %copy-done.3, bf16[4,512,8,64]{1,3,2,0:T(8,128)(2,1)} %bitcast.48, bf16[4,16,8,64]{3,2,1,0:T(8,128)(2,1)S(1)} %reshape.230, pred[4,512]{1,0:T(4,128)(4,1)S(1)} %get-tuple-element.90), kind=kOutput, calls=%fused_computation.96 | convolution fusion | flops 34602496 | bytes 3280896 | tf_op jit(solution)/shard_map/sphd,skhd->shpk/dot_general | solution.py:150
  56.0 0.3 fusion.17
  56.4 0.5 broadcast.155
  57.0 0.7 reduce.2
  57.7 0.7 reshape.243
  58.3 3.4 %all-to-all-start.2 = ((f32[4,1,128]{2,1,0:T(1,128)}), f32[4,1,128]{2,1,0:T(1,128)S(1)}, u32[]{:S(2)}, u32[]{:S(2)}) async-start(f32[4,1,128]{2,1,0:T(1,128)} %reshape.243), calls=%async_computation.2 | async-start | bytes 4096 | tf_op jit(solution)/shard_map/all_to_all | solution.py:162
  61.8 2.3 %convolution_bitcast_fusion = f32[4,16,8,64]{3,1,2,0:T(8,128)S(1)} fusion(bf16[4,512,8,64]{1,3,2,0:T(8,128)(2,1)} %bitcast.47, f32[4,8,16,512]{3,2,1,0:T(8,128)S(1)} %get-tuple-element.95, f32[4,8,16]{2,1,0:T(8,128)S(1)} %get-tuple-element.94, pred[4,512]{1,0:T(4,128)(4,1)S(1)} %get-tuple-element.90), kind=kOutput, calls=%fused_computation.21 | convolution fusion | flops 34340864 | bytes 3280896 | tf_op jit(solution)/shard_map/shpk,skhd->sphd/dot_general | solution.py:52
  64.1 3.2 %convolution_convert_fusion = bf16[4,512,1024]{2,1,0:T(8,128)(2,1)} fusion(bf16[4,16,512]{2,1,0:T(8,128)(2,1)S(1)} %bitcast.50, bf16[4,16,512]{2,1,0:T(8,128)(2,1)S(1)} %bitcast.49, s32[4,512]{1,0:T(4,128)S(1)} %broadcast_subtract_fusion), kind=kOutput, calls=%fused_computation.6 | convolution fusion | flops 69500928 | bytes 4333568 | tf_op jit(solution)/shard_map/skp,spc->skc/dot_general | solution.py:210
  67.3 0.2 fusion.56
  67.6 0.2 convolution_bitcast_fusion.1
  68.2 0.7 reduce.4
  68.9 0.7 reshape.241
  69.6 5.1 %all-to-all-start.1 = ((f32[4,1,128]{2,1,0:T(1,128)}), f32[4,1,128]{2,1,0:T(1,128)S(1)}, u32[]{:S(2)}, u32[]{:S(2)}) async-start(f32[4,1,128]{2,1,0:T(1,128)} %reshape.241), calls=%async_computation.1 | async-start | bytes 4096 | tf_op jit(solution)/shard_map/all_to_all | solution.py:161
  75.0 0.8 broadcast_in_dim_reshape_reshape.4
  75.8 0.6 reduce.3
  76.6 3.6 %all-to-all-done.1 = f32[4,1,128]{2,1,0:T(1,128)S(1)} async-done(((f32[4,1,128]{2,1,0:T(1,128)}), f32[4,1,128]{2,1,0:T(1,128)S(1)}, u32[]{:S(2)}, u32[]{:S(2)}) %all-to-all-start.1) | async-done | bytes 2080 | tf_op jit(solution)/shard_map/all_to_all | solution.py:161
  80.1 3.3 %all-to-all-start = ((f32[1,64,512]{2,0,1:T(1,128)}), f32[1,64,512]{2,0,1:T(1,128)S(1)}, u32[]{:S(2)}, u32[]{:S(2)}) async-start(f32[1,64,512]{2,0,1:T(1,128)} %broadcast_in_dim_reshape_reshape.4), calls=%async_computation | async-start | bytes 262144 | tf_op jit(solution)/shard_map/all_to_all | solution.py:163
  83.5 0.6 reduce.5
  85.2 4.2 %all-to-all-done = f32[1,64,512]{2,0,1:T(1,128)S(1)} async-done(((f32[1,64,512]{2,0,1:T(1,128)}), f32[1,64,512]{2,0,1:T(1,128)S(1)}, u32[]{:S(2)}, u32[]{:S(2)}) %all-to-all-start) | async-done | bytes 131104 | tf_op jit(solution)/shard_map/all_to_all | solution.py:163
  90.1 13.1 %all_gather.3 = bf16[64,512]{1,0:T(8,128)(2,1)S(1)} all-gather(bf16[16,512]{1,0:T(8,128)(2,1)S(1)} %multiply_convert_fusion.2), channel_id=1, replica_groups=mesh['dp'=4,'kv'=4,'tp'=2] {'kv'}, dimensions={0}, use_global_device_ids=true | all-gather | bytes 81920 | tf_op jit(solution)/shard_map/all_gather | solution.py:197
  103.2 0.8 convolution_convert_fusion.1
  104.1 4.4 %slice_select_fusion = (bf16[4,512,512]{2,1,0:T(8,128)(2,1)}, bf16[4,512,512]{2,1,0:T(8,128)(2,1)}) fusion(bf16[4,512,512]{2,1,0:T(8,128)(2,1)S(1)} %copy-done.2, bf16[4,512,1024]{2,1,0:T(8,128)(2,1)} %convolution_convert_fusion, pred[4,512]{1,0:T(4,128)(4,1)S(1)} %fusion.32, bf16[4,512,512]{2,1,0:T(8,128)(2,1)} %param.30), kind=kLoop, calls=%fused_computation.7 | loop fusion | flops 2097152 | bytes 12584960 | tf_op jit(solution)/shard_map/jit(_where)/select_n | solution.py:215
  108.5 12.4 %all-reduce.6.cloned.1.call-done = bf16[4,16,512]{2,1,0:T(8,128)(2,1)} async-done(((bf16[4,16,512]{2,1,0:T(8,128)(2,1)}), bf16[4,16,512]{2,1,0:T(8,128)(2,1)}) %all-reduce.6.cloned.1.call-update) | async-done | bytes 65552 | tf_op jit(solution)/shard_map/psum | solution.py:199
  121.0 1.5 %copy.192 = bf16[4,16,512]{2,1,0:T(8,128)(2,1)} copy(bf16[4,16,512]{2,1,0:T(8,128)(2,1)} %all-reduce.6.cloned.1.call-done) | data formatting | bytes 131072
  (122 shorter events, 5.9 us)
Async XLA Ops:
  7.2 96.0 %copy-start = (bf16[512,512]{1,0:T(8,128)(2,1)S(1)}, bf16[512,512]{1,0:T(8,128)(2,1)}, u32[]{:S(2)}) copy-start(bf16[512,512]{1,0:T(8,128)(2,1)} %param.29) | copy-start | bytes 1572868
  7.2 43.8 %all-reduce.4.cloned.1.call-start = ((), (), s32[]{:S(2)}) async-start(), calls=%async_computation.3 | async-start | bytes 786432 | tf_op jit(solution)/shard_map/psum | solution.py:130
  8.1 2.7 %copy-start.4 = (bf16[4,16,512]{2,1,0:T(8,128)(2,1)S(1)}, bf16[4,16,512]{2,1,0:T(8,128)(2,1)}, u32[]{:S(2)}) copy-start(bf16[4,16,512]{2,1,0:T(8,128)(2,1)} %param.19) | copy-start | bytes 196612
  8.2 2.9 %copy-start.11 = (s32[4]{0:T(128)S(1)}, s32[4]{0:T(128)}, u32[]{:S(2)}) copy-start(s32[4]{0:T(128)} %param.33) | copy-start | bytes 52
  8.2 2.9 %copy-start.12 = (s32[4]{0:T(128)S(1)}, s32[4]{0:T(128)}, u32[]{:S(2)}) copy-start(s32[4]{0:T(128)} %param.34) | copy-start | bytes 52
  8.2 3.0 %copy-start.6 = (s32[4,16]{1,0:T(4,128)S(1)}, s32[4,16]{1,0:T(4,128)}, u32[]{:S(2)}) copy-start(s32[4,16]{1,0:T(4,128)} %param.35) | copy-start | bytes 772
  8.2 7.3 %copy-start.3 = (f32[4,8,512]{2,1,0:T(8,128)S(1)}, f32[4,8,512]{2,1,0:T(8,128)}, u32[]{:S(2)}) copy-start(f32[4,8,512]{2,1,0:T(8,128)} %param.32) | copy-start | bytes 196612
  8.2 28.7 %copy-start.7 = (f32[16]{0:T(128)S(1)}, f32[16]{0:T(128)}, u32[]{:S(2)}) copy-start(f32[16]{0:T(128)} %param.25) | copy-start | bytes 196
  8.2 28.8 %copy-start.8 = (f32[64]{0:T(128)S(1)}, f32[64]{0:T(128)}, u32[]{:S(2)}) copy-start(f32[64]{0:T(128)} %param.26) | copy-start | bytes 772
  8.2 28.8 %copy-start.9 = (f32[64]{0:T(128)S(1)}, f32[64]{0:T(128)}, u32[]{:S(2)}) copy-start(f32[64]{0:T(128)} %param.27) | copy-start | bytes 772
  8.2 28.9 %copy-start.10 = (f32[64]{0:T(128)S(1)}, f32[64]{0:T(128)}, u32[]{:S(2)}) copy-start(f32[64]{0:T(128)} %param.28) | copy-start | bytes 772
  37.4 6.7 %copy-start.5 = (f32[4,16,8]{1,2,0:T(8,128)}, f32[4,16,8]{1,2,0:T(8,128)S(1)}, u32[]{:S(2)}) copy-start(f32[4,16,8]{1,2,0:T(8,128)S(1)} %copy.148) | copy-start | bytes 6148
  37.4 4.3 %copy-start.1 = (bf16[4,512,512]{2,1,0:T(8,128)(2,1)S(1)}, bf16[4,512,512]{2,1,0:T(8,128)(2,1)}, u32[]{:S(2)}) copy-start(bf16[4,512,512]{2,1,0:T(8,128)(2,1)} %param.31) | copy-start | bytes 6291460
  58.3 11.2 %all-to-all-start.2 = ((f32[4,1,128]{2,1,0:T(1,128)}), f32[4,1,128]{2,1,0:T(1,128)S(1)}, u32[]{:S(2)}, u32[]{:S(2)}) async-start(f32[4,1,128]{2,1,0:T(1,128)} %reshape.243), calls=%async_computation.2 | async-start | bytes 4096 | tf_op jit(solution)/shard_map/all_to_all | solution.py:162
  69.6 10.6 %all-to-all-start.1 = ((f32[4,1,128]{2,1,0:T(1,128)}), f32[4,1,128]{2,1,0:T(1,128)S(1)}, u32[]{:S(2)}, u32[]{:S(2)}) async-start(f32[4,1,128]{2,1,0:T(1,128)} %reshape.241), calls=%async_computation.1 | async-start | bytes 4096 | tf_op jit(solution)/shard_map/all_to_all | solution.py:161
  75.0 29.1 %copy-start.2 = (bf16[4,512,512]{2,1,0:T(8,128)(2,1)S(1)}, bf16[4,512,512]{2,1,0:T(8,128)(2,1)}, u32[]{:S(2)}) copy-start(bf16[4,512,512]{2,1,0:T(8,128)(2,1)} %param.31) | copy-start | bytes 6291460
  80.1 9.2 %all-to-all-start = ((f32[1,64,512]{2,0,1:T(1,128)}), f32[1,64,512]{2,0,1:T(1,128)S(1)}, u32[]{:S(2)}, u32[]{:S(2)}) async-start(f32[1,64,512]{2,0,1:T(1,128)} %broadcast_in_dim_reshape_reshape.4), calls=%async_computation | async-start | bytes 262144 | tf_op jit(solution)/shard_map/all_to_all | solution.py:163
  83.5 37.5 %all-reduce.6.cloned.1.call-start = ((), (), s32[]{:S(2)}) async-start(), calls=%async_computation.4 | async-start | bytes 131072 | tf_op jit(solution)/shard_map/psum | solution.py:199
Sparse Core Ops, SparseCore 0:
  11.0 39.9 all-reduce.3
  104.2 16.7 all-reduce.5
where the time goes:
time: 130 us; the launch traced here: 129 us
  blocking collectives  33.6 us (26%)
  waiting for transfers between devices  27 us (21%)
  matrix products  16.2 us (12%)
  local copies, waits for them, and re-layouts  14.8 us (11%)
  between operations  14.5 us (11%)
  starting transfers between devices  11.9 us (9%)
  other arithmetic  10.9 us (8%)
    psum x1, blocking collectives, shards(): lax.psum((jnp.dot(scaled, w_joined, preferred_element_type=jnp.float32),...  20.4 us
    all_gather x1, blocking collectives, shards(): normed = lax.all_gather(own_normed, 'kv', axis=0, tiled=True)  13.1 us
    psum x1, waiting for transfers between devices, shards(): layer_out = lax.psum(out_term.astype(jnp.bfloat16), 'tp')  12.4 us
    unnamed x34, local copies, waits for them, and re-layouts  10.3 us
    psum x1, waiting for transfers between devices, shards(): lax.psum((jnp.dot(scaled, w_joined, preferred_element_type=jnp.float32),...  6.72 us
    all_to_all x1, starting transfers between devices, shards(): lax.all_to_all(flat_max[None], 'kv', split_axis=1, concat_axis=0, tiled=T...  5.09 us
    select_n x1, other arithmetic, shards(): new_values = jnp.where(hit_rows, written[..., head_width:], value_cache)  4.45 us
    all_to_all x1, waiting for transfers between devices, shards(): lax.all_to_all(flat_sum[None], 'kv', split_axis=1, concat_axis=0, tiled=T...  4.2 us
  transfers between devices with their start and end apart: 5, of which 4 were waited for; matrix products, arithmetic and copies ran while one was open for 22% of the time, Pallas kernels for 0%

commit v1 on v0

--- a/solution.py
+++ b/solution.py
@@ -1,6 +1,10 @@
+import functools
+
 import jax
 import jax.numpy as jnp
 from jax import lax
+from jax.experimental import pallas as pl
+from jax.experimental.pallas import tpu as pltpu
 from jax.sharding import PartitionSpec as P
 
 EPSILON = 1e-06
@@ -216,6 +220,584 @@
     return (layer_out, new_keys, new_values, log_own)
 
 
+MESH = pl.DeviceIdType.MESH
+LANES = 128
+
+
+def tile_head_norm(rows, gain_row, head_size):
+    lane = lax.broadcasted_iota(jnp.int32, (rows.shape[0], LANES), 1)
+    low = lane < head_size
+    parts = []
+    for start in range(0, rows.shape[1], LANES):
+        part = rows[:, start : start + LANES]
+        square = part * part
+        first = jnp.sum(jnp.where(low, square, 0.0), axis=1, keepdims=True) / head_size
+        second = jnp.sum(jnp.where(low, 0.0, square), axis=1, keepdims=True) / head_size
+        parts.append(part * lax.rsqrt(jnp.where(low, first, second) + EPSILON) * gain_row)
+    return jnp.concatenate(parts, axis=1)
+
+
+def spread_heads(stats, offset, heads, head_size):
+    lane = lax.broadcasted_iota(jnp.int32, (stats.shape[0], LANES), 1)
+    return jnp.concatenate(
+        [
+            jnp.where(
+                lane < head_size,
+                stats[:, offset + head : offset + head + 1],
+                stats[:, offset + head + 1 : offset + head + 2],
+            )
+            for head in range(0, heads, 2)
+        ],
+        axis=1,
+    )
+
+
+def attend_rows(queries, keys, values, adjust, live, heads, head_size, scale):
+    props = queries.shape[0]
+    quad = 4
+    width = quad * head_size
+    row_head = lax.broadcasted_iota(jnp.int32, (quad * props, width), 0) // props
+    col_head = lax.broadcasted_iota(jnp.int32, (quad * props, width), 1) // head_size
+    own = (row_head == col_head).astype(jnp.float32).astype(jnp.bfloat16)
+    lane = lax.broadcasted_iota(jnp.int32, (props, LANES), 1)
+    tiles, peaks, totals = [], [], []
+    for group in range(heads // quad):
+        columns = slice(group * width, (group + 1) * width)
+        stacked = jnp.concatenate([queries[:, columns]] * quad, axis=0) * own
+        scores = lax.dot_general(
+            stacked, keys[:, columns], (((1,), (1,)), ((), ())), preferred_element_type=jnp.float32
+        )
+        weights = []
+        for inner in range(quad):
+            head = group * quad + inner
+            part = scores[inner * props : (inner + 1) * props] * scale - adjust(head)
+            part = jnp.where(live, part, MASKED)
+            peak = jnp.max(part, axis=1, keepdims=True)
+            weight = jnp.where(live, jnp.exp(part - peak), 0.0)
+            peaks.append(peak)
+            totals.append(jnp.sum(weight, axis=1, keepdims=True))
+            weights.append(weight.astype(jnp.bfloat16))
+        summed = jnp.dot(
+            jnp.concatenate(weights, axis=0), values[:, columns], preferred_element_type=jnp.float32
+        )
+        for pair in range(quad // 2):
+            cols = slice(pair * LANES, (pair + 1) * LANES)
+            first = summed[2 * pair * props : (2 * pair + 1) * props, cols]
+            second = summed[(2 * pair + 1) * props : (2 * pair + 2) * props, cols]
+            tiles.append(jnp.where(lane < head_size, first, second))
+    return jnp.concatenate(tiles, axis=1), peaks, totals
+
+
+def pack_stats(columns, props):
+    lane = lax.broadcasted_iota(jnp.int32, (props, LANES), 1)
+    stats = jnp.zeros((props, LANES), jnp.float32)
+    for index, column in enumerate(columns):
+        stats = jnp.where(lane == index, column, stats)
+    return stats
+
+
+def layer_kernel(
+    sizes,
+    lengths,
+    accepted,
+    parents,
+    tokens,
+    norm_gain,
+    w_query,
+    w_key,
+    w_value,
+    w_forget,
+    forget_bias,
+    query_gain,
+    key_gain,
+    head_gain,
+    w_out,
+    key_cache,
+    value_cache,
+    gate_cache,
+    out_layer,
+    out_rows,
+    out_gates,
+    tok_v,
+    norm_v,
+    wq_v,
+    wk_v,
+    wv_v,
+    wf_v,
+    bias_v,
+    qgain_v,
+    kgain_v,
+    hgain_v,
+    wo_v,
+    kc_v,
+    vc_v,
+    gc_v,
+    send_q,
+    send_kv,
+    got_q,
+    got_kv,
+    all_q,
+    all_gates,
+    all_kv,
+    send_part,
+    got_part,
+    all_normed,
+    term_own,
+    term_other,
+    load_sem,
+    sent_sem,
+    came_sem,
+    pair_sem,
+):
+    n, heads, head_size, full_width = sizes
+    me = lax.axis_index("kv")
+    core = lax.axis_index("tp")
+    seqs, props, width_in = tok_v.shape
+    head_width = heads * head_size
+    pos_dev = kc_v.shape[1]
+    rows_all = seqs * props
+    scale = head_size ** (-0.5)
+    order = sorted(range(1, n), key=lambda step: abs(2 * step - n))
+
+    forget_rows = pl.ds(pl.multiple_of(me * width_in, width_in), width_in)
+    loads = {}
+    for index, (name, source, target) in enumerate(
+        (
+            ("tokens", tokens, tok_v),
+            ("norm", norm_gain, norm_v),
+            ("wq", w_query, wq_v),
+            ("wf", w_forget.at[forget_rows], wf_v),
+            ("bias", forget_bias, bias_v),
+            ("qgain", query_gain, qgain_v),
+            ("kgain", key_gain, kgain_v),
+            ("hgain", head_gain, hgain_v),
+            ("wk", w_key, wk_v),
+            ("wv", w_value, wv_v),
+            ("gates", gate_cache, gc_v),
+            ("keys", key_cache, kc_v),
+            ("values", value_cache, vc_v),
+            ("wo", w_out, wo_v),
+        )
+    ):
+        loads[name] = pltpu.make_async_copy(source, target, load_sem.at[index])
+        loads[name].start()
+
+    barrier = pltpu.get_barrier_semaphore()
+    for step in order:
+        pl.semaphore_signal(
+            barrier, inc=1, device_id={"kv": lax.rem(me + step, n)}, device_id_type=MESH
+        )
+    pl.semaphore_signal(barrier, inc=1, device_id={"tp": 1 - core}, device_id_type=MESH)
+
+    sent = []
+
+    def push(phase, step, source, target):
+        peer = lax.rem(me + step, n)
+        copy = pltpu.make_async_remote_copy(
+            src_ref=source(peer),
+            dst_ref=target.at[me],
+            send_sem=sent_sem.at[phase, step],
+            recv_sem=came_sem.at[phase, me],
+            device_id={"kv": peer},
+            device_id_type=MESH,
+        )
+        copy.start()
+        sent.append(copy)
+
+    def arrive(phase, step, target):
+        peer = lax.rem(me + step, n)
+        pltpu.make_async_remote_copy(
+            src_ref=target.at[peer],
+            dst_ref=target.at[peer],
+            send_sem=sent_sem.at[phase, step],
+            recv_sem=came_sem.at[phase, peer],
+            device_id={"kv": peer},
+            device_id_type=MESH,
+        ).wait_recv()
+
+    loads["tokens"].wait()
+    loads["norm"].wait()
+    flat = tok_v[...].astype(jnp.float32).reshape(rows_all, width_in)
+    squares = jnp.sum(flat * flat, axis=1, keepdims=True)
+    scaled = (flat * norm_v[...]).astype(jnp.bfloat16)
+    loads["wq"].wait()
+    loads["wf"].wait()
+    send_q[:, :, :head_width] = jnp.dot(
+        scaled, wq_v[...], preferred_element_type=jnp.float32
+    ).reshape(seqs, props, head_width)
+    gate_part = jnp.dot(scaled, wf_v[...], preferred_element_type=jnp.float32)
+    gate_heads = gate_part.shape[1]
+    send_q[:, :, head_width:] = jnp.broadcast_to(squares, (rows_all, LANES)).reshape(
+        seqs, props, LANES
+    )
+    send_q[:, :, head_width : head_width + gate_heads] = gate_part.reshape(seqs, props, gate_heads)
+    pl.semaphore_wait(barrier, n)
+    for step in order:
+        push(0, step, lambda peer: send_q.at[peer], got_q)
+
+    loads["wk"].wait()
+    send_kv[:, :, :head_width] = jnp.dot(
+        scaled, wk_v[...], preferred_element_type=jnp.float32
+    ).reshape(seqs, props, head_width)
+    loads["wv"].wait()
+    send_kv[:, :, head_width:] = jnp.dot(
+        scaled, wv_v[...], preferred_element_type=jnp.float32
+    ).reshape(seqs, props, head_width)
+
+    row = lax.broadcasted_iota(jnp.int32, (LANES, LANES), 0)
+    column = lax.broadcasted_iota(jnp.int32, (LANES, LANES), 1)
+    eye = (row == column).astype(jnp.float32)
+    target_column = jnp.full((LANES, LANES), -1, jnp.int32)
+    for prop in range(props):
+        target_column = jnp.where(row == prop, parents[me, prop], target_column)
+    power = (target_column == column).astype(jnp.float32)
+    ancestors = eye + power
+    reach = 2
+    while reach < props:
+        half = power.astype(jnp.bfloat16)
+        power = jnp.dot(half, half, preferred_element_type=jnp.float32)
+        ancestors = ancestors + jnp.dot(
+            ancestors.astype(jnp.bfloat16),
+            power.astype(jnp.bfloat16),
+            preferred_element_type=jnp.float32,
+        )
+        reach *= 2
+    for name in ("bias", "qgain", "kgain", "hgain"):
+        loads[name].wait()
+    gain_q = jnp.concatenate([qgain_v[...]] * (LANES // head_size), axis=1)
+    gain_k = jnp.concatenate([kgain_v[...]] * (LANES // head_size), axis=1)
+    gain_h = jnp.concatenate([hgain_v[...]] * (LANES // head_size), axis=1)
+
+    for step in order:
+        arrive(0, step, got_q)
+    raw = send_q[me]
+    for step in range(1, n):
+        raw = raw + got_q[lax.rem(me + step, n)]
+    small = raw[:, head_width:]
+    inverse = lax.rsqrt(small[:, gate_heads : gate_heads + 1] / full_width + EPSILON)
+    all_q[me] = tile_head_norm(raw[:, :head_width] * inverse, gain_q, head_size).astype(
+        jnp.bfloat16
+    )
+    for step in order:
+        push(1, step, lambda peer: all_q.at[me], all_q)
+    logits = small[:, :gate_heads] * inverse + bias_v[...]
+    logs = -(jnp.maximum(-logits, 0.0) + jnp.log1p(jnp.exp(-jnp.abs(logits))))
+    logs = jnp.where(core == 0, logs[:, :heads], logs[:, heads:])
+    all_gates[me] = jnp.zeros((props, LANES), jnp.float32)
+    all_gates[me, :, :heads] = logs
+    for step in order:
+        push(2, step, lambda peer: send_kv.at[peer], got_kv)
+    for step in order:
+        push(3, step, lambda peer: all_gates.at[me], all_gates)
+
+    lane_pos = me * pos_dev + lax.broadcasted_iota(jnp.int32, (props, pos_dev), 1)
+    loads["gates"].wait()
+    loads["keys"].wait()
+    loads["values"].wait()
+    for step in [0] + order:
+        seq = lax.rem(me + step, n)
+        if step:
+            arrive(1, step, all_q)
+        base = lengths[seq] + accepted[seq]
+        gate_rows = gc_v[seq]
+        hit = lane_pos == base - 1
+        total, peaks, totals = attend_rows(
+            all_q[seq],
+            kc_v[seq],
+            vc_v[seq],
+            lambda head: gate_rows[head : head + 1],
+            lane_pos < base,
+            heads,
+            head_size,
+            scale,
+        )
+        edges = [
+            jnp.sum(
+                jnp.where(hit[:1], gate_rows[head : head + 1], 0.0), axis=1, keepdims=True
+            )
+            for head in range(heads)
+        ]
+        send_part[seq, :, :head_width] = total
+        send_part[seq, :, head_width:] = pack_stats(peaks + totals + edges, props)
+        if step:
+            push(4, step, lambda peer: send_part.at[peer], got_part)
+
+    for step in order:
+        arrive(2, step, got_kv)
+    raw = send_kv[me]
+    for step in range(1, n):
+        raw = raw + got_kv[lax.rem(me + step, n)]
+    raw = raw * inverse
+    keys_own = tile_head_norm(raw[:, :head_width], gain_k, head_size).astype(jnp.bfloat16)
+    values_own = raw[:, head_width:].astype(jnp.bfloat16)
+    all_kv[me, :, :head_width] = keys_own
+    all_kv[me, :, head_width:] = values_own
+    for step in order:
+        push(5, step, lambda peer: all_kv.at[me], all_kv)
+
+    padding = jnp.zeros((LANES - props, head_width), jnp.bfloat16)
+    log_tile = jnp.concatenate(
+        [all_gates[me], jnp.zeros((LANES - props, LANES), jnp.float32)], axis=0
+    )
+    path_sum = jnp.dot(ancestors, log_tile, precision=lax.Precision.HIGHEST)
+    on_diagonal = row == column
+    tree_sum, tree_peaks, tree_totals = attend_rows(
+        all_q[me],
+        jnp.concatenate([keys_own, padding], axis=0),
+        jnp.concatenate([values_own, padding], axis=0),
+        lambda head: jnp.sum(
+            jnp.where(on_diagonal, path_sum[:, head : head + 1], 0.0), axis=0, keepdims=True
+        ),
+        ancestors[:props] > 0.5,
+        heads,
+        head_size,
+        scale,
+    )
+    tree_stats = pack_stats(tree_peaks + tree_totals, props)
+
+    for step in order:
+        arrive(4, step, got_part)
+    parts = [send_part[me]] + [got_part[lax.rem(me + step, n)] for step in range(1, n)]
+    edge = functools.reduce(jnp.add, [part[:, head_width:] for part in parts])
+    tops = [spread_heads(part[:, head_width:], 0, heads, head_size) for part in parts]
+    sums = [spread_heads(part[:, head_width:], heads, heads, head_size) for part in parts]
+    numbers = [part[:, :head_width] for part in parts]
+    tops.append(
+        spread_heads(tree_stats, 0, heads, head_size)
+        - spread_heads(edge, 2 * heads, heads, head_size)
+    )
+    sums.append(spread_heads(tree_stats, heads, heads, head_size))
+    numbers.append(tree_sum)
+    top = functools.reduce(jnp.maximum, tops)
+    factors = [jnp.exp(each - top) for each in tops]
+    weighted = functools.reduce(jnp.add, [x * y for x, y in zip(numbers, factors)])
+    row_total = functools.reduce(jnp.add, [x * y for x, y in zip(sums, factors)])
+    all_normed[me] = tile_head_norm(weighted / row_total, gain_h, head_size).astype(jnp.bfloat16)
+    for step in order:
+        push(6, step, lambda peer: all_normed.at[me], all_normed)
+    loads["wo"].wait()
+    for step in order:
+        arrive(6, step, all_normed)
+    term_own[...] = jnp.dot(
+        all_normed[...].reshape(rows_all, head_width),
+        wo_v[...],
+        preferred_element_type=jnp.float32,
+    ).astype(jnp.bfloat16)
+    pair = pltpu.make_async_remote_copy(
+        src_ref=term_own,
+        dst_ref=term_other,
+        send_sem=pair_sem.at[0],
+        recv_sem=pair_sem.at[1],
+        device_id={"tp": 1 - core},
+        device_id_type=MESH,
+    )
+    pair.start()
+    for step in order:
+        arrive(3, step, all_gates)
+    for step in order:
+        arrive(5, step, all_kv)
+    out_gates[...] = all_gates[:, :, :heads]
+    out_rows[...] = all_kv[...]
+    pair.wait()
+    joined = term_own[...].astype(jnp.float32) + term_other[...].astype(jnp.float32)
+    out_layer[...] = joined.astype(jnp.bfloat16).reshape(out_layer.shape)
+    for copy in sent:
+        copy.wait_send()
+
+
+def write_kernel(
+    lengths,
+    accepted,
+    layer_in,
+    rows_in,
+    gates_in,
+    key_cache,
+    value_cache,
+    layer_out,
+    new_keys,
+    new_values,
+    gates_out,
+    kc_v,
+    vc_v,
+    in_sem,
+    out_sem,
+):
+    seqs, pos_dev, head_width = kc_v.shape
+    props = rows_in.shape[1]
+    window = 2 * props
+    start = lax.axis_index("kv") * pos_dev
+    caches = ((key_cache, kc_v, new_keys), (value_cache, vc_v, new_values))
+    loads = [
+        [
+            pltpu.make_async_copy(source.at[seq], held.at[seq], in_sem.at[side, seq])
+            for side, (source, held, _) in enumerate(caches)
+        ]
+        for seq in range(seqs)
+    ]
+    for pair in loads:
+        for copy in pair:
+            copy.start()
+    layer_out[...] = layer_in[...]
+    gates_out[...] = gates_in[...]
+    slot = lax.broadcasted_iota(jnp.int32, (window, props), 0)
+    prop = lax.broadcasted_iota(jnp.int32, (window, props), 1)
+    line = lax.broadcasted_iota(jnp.int32, (window, head_width), 0)
+    stores = []
+    for seq in range(seqs):
+        offset = lengths[seq] + accepted[seq] - start
+        inside = jnp.clip(offset, 0, pos_dev - 1)
+        lower = jnp.minimum(inside // props * props, pos_dev - window)
+        rows = pl.ds(pl.multiple_of(lower, props), window)
+        placing = (slot + lower - offset == prop).astype(jnp.float32).astype(jnp.bfloat16)
+        place = line + lower - offset
+        hit = (place >= 0) & (place < props)
+        for side, (_, held, target) in enumerate(caches):
+            fresh = jnp.dot(
+                placing,
+                rows_in[seq, :, side * head_width : (side + 1) * head_width],
+                preferred_element_type=jnp.float32,
+            )
+            loads[seq][side].wait()
+            kept = held[seq, rows, :].astype(jnp.float32)
+            held[seq, rows, :] = jnp.where(hit, fresh, kept).astype(jnp.bfloat16)
+            copy = pltpu.make_async_copy(held.at[seq], target.at[seq], out_sem.at[side, seq])
+            copy.start()
+            stores.append(copy)
+    for copy in stores:
+        copy.wait()
+
+
+def fused_shards(
+    tokens,
+    norm_gain,
+    w_query,
+    w_key,
+    w_value,
+    w_forget,
+    forget_bias,
+    query_gain,
+    key_gain,
+    head_gain,
+    w_out,
+    key_cache,
+    value_cache,
+    gate_cache,
+    lengths,
+    accepted,
+    parents,
+    n,
+):
+    seqs, props, width_in = tokens.shape
+    pos_dev, head_width = key_cache.shape[1:]
+    heads = gate_cache.shape[1]
+    head_size = head_width // heads
+    width_out = w_out.shape[1]
+    bf16, f32 = jnp.bfloat16, jnp.float32
+    smem = pl.BlockSpec(memory_space=pltpu.SMEM)
+    vmem = pl.BlockSpec(memory_space=pltpu.VMEM)
+    any_space = pl.BlockSpec(memory_space=pl.ANY)
+    line = lambda vector: vector.reshape(1, -1)
+    operands = (
+        tokens,
+        line(norm_gain),
+        w_query,
+        w_key,
+        w_value,
+        w_forget,
+        line(forget_bias),
+        line(query_gain),
+        line(key_gain),
+        line(head_gain),
+        w_out,
+        key_cache,
+        value_cache,
+        gate_cache,
+    )
+    part_width = head_width + LANES
+    scratch = [
+        pltpu.VMEM(tokens.shape, bf16),
+        pltpu.VMEM((1, width_in), f32),
+        pltpu.VMEM(w_query.shape, bf16),
+        pltpu.VMEM(w_key.shape, bf16),
+        pltpu.VMEM(w_value.shape, bf16),
+        pltpu.VMEM((width_in, w_forget.shape[1]), bf16),
+        pltpu.VMEM((1, forget_bias.shape[0]), f32),
+        pltpu.VMEM((1, head_size), f32),
+        pltpu.VMEM((1, head_size), f32),
+        pltpu.VMEM((1, head_size), f32),
+        pltpu.VMEM(w_out.shape, bf16),
+        pltpu.VMEM(key_cache.shape, bf16),
+        pltpu.VMEM(value_cache.shape, bf16),
+        pltpu.VMEM(gate_cache.shape, f32),
+        pltpu.VMEM((seqs, props, part_width), f32),
+        pltpu.VMEM((seqs, props, 2 * head_width), f32),
+        pltpu.VMEM((n, props, part_width), f32),
+        pltpu.VMEM((n, props, 2 * head_width), f32),
+        pltpu.VMEM((n, props, head_width), bf16),
+        pltpu.VMEM((n, props, LANES), f32),
+        pltpu.VMEM((n, props, 2 * head_width), bf16),
+        pltpu.VMEM((seqs, props, part_width), f32),
+        pltpu.VMEM((n, props, part_width), f32),
+        pltpu.VMEM((n, props, head_width), bf16),
+        pltpu.VMEM((seqs * props, width_out), bf16),
+        pltpu.VMEM((seqs * props, width_out), bf16),
+        pltpu.SemaphoreType.DMA((14,)),
+        pltpu.SemaphoreType.DMA((7, n)),
+        pltpu.SemaphoreType.DMA((7, n)),
+        pltpu.SemaphoreType.DMA((2,)),
+    ]
+    layer, rows, gates = pl.pallas_call(
+        functools.partial(layer_kernel, (n, heads, head_size, w_forget.shape[0])),
+        out_shape=(
+            jax.ShapeDtypeStruct((seqs, props, width_out), bf16),
+            jax.ShapeDtypeStruct((seqs, props, 2 * head_width), bf16),
+            jax.ShapeDtypeStruct((seqs, props, heads), f32),
+        ),
+        in_specs=[smem] * 3 + [any_space] * len(operands),
+        out_specs=(vmem, vmem, vmem),
+        scratch_shapes=scratch,
+        compiler_params=pltpu.CompilerParams(collective_id=0, has_side_effects=True),
+        name="layer",
+    )(lengths, accepted, parents, *operands)
+    return pl.pallas_call(
+        write_kernel,
+        out_shape=(
+            jax.ShapeDtypeStruct(layer.shape, bf16),
+            jax.ShapeDtypeStruct(key_cache.shape, bf16),
+            jax.ShapeDtypeStruct(value_cache.shape, bf16),
+            jax.ShapeDtypeStruct(gates.shape, f32),
+        ),
+        in_specs=[smem, smem, vmem, vmem, vmem, any_space, any_space],
+        out_specs=(vmem, any_space, any_space, vmem),
+        scratch_shapes=[
+            pltpu.VMEM(key_cache.shape, bf16),
+            pltpu.VMEM(value_cache.shape, bf16),
+            pltpu.SemaphoreType.DMA((2, seqs)),
+            pltpu.SemaphoreType.DMA((2, seqs)),
+        ],
+        name="write",
+    )(lengths, accepted, layer, rows, gates, key_cache, value_cache)
+
+
+def pick_shards(n, cores):
+    def chosen(*arrays):
+        tokens, key_cache, gate_cache = arrays[0], arrays[11], arrays[13]
+        heads = gate_cache.shape[1]
+        fits = (
+            tokens.shape[0] == n
+            and n > 1
+            and cores == 2
+            and tokens.shape[1] == 16
+            and tokens.shape[2] % LANES == 0
+            and key_cache.shape[2] == 64 * heads
+            and heads % 4 == 0
+            and 3 * heads <= LANES
+        )
+        return fused_shards(*arrays, n) if fits else shards(*arrays)
+
+    return chosen
+
+
 def solution(mesh):
     placed = (
         P("dp", None, "kv"),
@@ -237,7 +819,7 @@
         P("dp", None),
     )
     return jax.shard_map(
-        shards,
+        pick_shards(mesh.shape["kv"], mesh.shape["tp"]),
         mesh=mesh,
         in_specs=placed,
         out_specs=(

time: 130 us -> 39.9 us (0.31)
  Pallas kernels: 0 us -> 35.7 us
  blocking collectives: 33.6 us -> 0 us
  waiting for transfers between devices: 27 us -> 0 us
  matrix products: 16.2 us -> 0 us
  between operations: 14.5 us -> 0.65 us
  starting transfers between devices: 11.9 us -> 0 us
  local copies, waits for them, and re-layouts: 14.8 us -> 3.28 us
  other arithmetic: 10.9 us -> 0 us
    pallas_call x0 -> x2, Pallas kernels: none -> 35.7 us  [the longest x1 30.5 us: fused_shards(): pl.pallas_call(functools.partial(layer_kernel, (n, heads, head_size, w_fo...]
    psum x1 -> x0, blocking collectives: 20.4 us -> none  [shards(): lax.psum((jnp.dot(scaled, w_joined, preferred_element_type=jnp.float32),...]
    psum x2 -> x0, waiting for transfers between devices: 19.2 us -> none  [the longest x1 12.4 us: shards(): layer_out = lax.psum(out_term.astype(jnp.bfloat16), 'tp')]
    dot_general x25 -> x0, matrix products: 16.2 us -> none  [the longest x16 3.67 us: extend(): jnp.einsum('sij,sjk->sik', step_matrix, ancestors, precision=lax.Precisio...]
    all_gather x1 -> x0, blocking collectives: 13.1 us -> none  [shards(): normed = lax.all_gather(own_normed, 'kv', axis=0, tiled=True)]
    all_to_all x3 -> x0, starting transfers between devices: 11.8 us -> none  [the longest x1 5.09 us: shards(): lax.all_to_all(flat_max[None], 'kv', split_axis=1, concat_axis=0, tiled=T...]
    unnamed x34 -> x1, local copies, waits for them, and re-layouts: 10.3 us -> 1.84 us
    all_to_all x3 -> x0, waiting for transfers between devices: 7.78 us -> none  [the longest x1 4.2 us: shards(): lax.all_to_all(flat_sum[None], 'kv', split_axis=1, concat_axis=0, tiled=T...]
  transfers between devices with their start and end apart: 5 -> 0, of which waited for: 4 -> 0; matrix products, arithmetic and copies ran while one was open for 22% -> 0% of each run, Pallas kernels for 0% -> 0%
where the time goes in v1:
time: 39.9 us; the launch traced here: 39.6 us
  Pallas kernels  35.7 us (89%)
  local copies, waits for them, and re-layouts  3.28 us (8%)
  between operations  0.65 us (2%)
    pallas_call x1, Pallas kernels, fused_shards(): pl.pallas_call(functools.partial(layer_kernel, (n, heads, head_size, w_fo...  30.5 us
    pallas_call x1, Pallas kernels, fused_shards(): pl.pallas_call(write_kernel, out_shape=(jax.ShapeDtypeStruct(layer.shape,...  5.12 us
    unnamed x1, local copies, waits for them, and re-layouts  1.84 us
    pallas_call x1, local copies, waits for them, and re-layouts, fused_shards(): pl.pallas_call(write_kernel, out_shape=(jax.ShapeDtypeStruct(layer.shape,...  1.44 us

profile of v1, /device:TPU:0, one launch (start us, length us, event | category | flops | bytes accessed | tf_op | source)
XLA Modules:
  0.0 39.6 jit_solution(9573656441286890413)
XLA Ops:
  0.6 1.8 %copy.21.w_forget = bf16[2048,16]{1,0:T(8,128)(2,1)} copy(bf16[2048,16]{0,1:T(8,128)(2,1)} %param.22) | data formatting | bytes 131072 | tf_op args[5]
  2.5 30.5 %layer.1 = (bf16[4,16,512]{2,1,0:T(8,128)(2,1)}, bf16[4,16,1024]{2,1,0:T(8,128)(2,1)}, f32[4,16,8]{2,1,0:T(8,128)}) custom-call(s32[4]{0:T(128)} %lengths.3, s32[4]{0:T(128)} %accepted.3, s32[4,16]{1,0:T(4,128)} %parents.1, bf16[4,16,512]{2,1,0:T(8,128)(2,1)} %tokens.1, f32[1,512]{1,0:T(1,128)} %bitcast.5, bf16[512,512]{1,0:T(8,128)(2,1)} %w_query.1, ...), custom_call_target="tpu_custom_call" | custom-call | tf_op jit(solution)/shard_map/layer/pallas_call | solution.py:749
  33.0 5.1 %write.1 = (bf16[4,16,512]{2,1,0:T(8,128)(2,1)}, bf16[4,512,512]{2,1,0:T(8,128)(2,1)}, bf16[4,512,512]{2,1,0:T(8,128)(2,1)}, f32[4,16,8]{2,1,0:T(8,128)}) custom-call(s32[4]{0:T(128)} %lengths.3, s32[4]{0:T(128)} %accepted.3, bf16[4,16,512]{2,1,0:T(8,128)(2,1)} %get-tuple-element.7.layer_in, bf16[4,16,1024]{2,1,0:T(8,128)(2,1)} %get-tuple-element.8.rows_in, ...), custom_call_target="tpu_custom_call" | custom-call | tf_op jit(solution)/shard_map/write/pallas_call | solution.py:762
  38.2 1.4 %copy.22 = f32[4,16,8]{1,2,0:T(8,128)} copy(f32[4,16,8]{2,1,0:T(8,128)} %get-tuple-element.13) | data formatting | bytes 4096 | tf_op jit(solution)/shard_map/write/pallas_call | solution.py:762

commit v2 on v1

--- a/solution.py
+++ b/solution.py
@@ -318,6 +318,8 @@
     out_layer,
     out_rows,
     out_gates,
+    kc_v,
+    vc_v,
     tok_v,
     norm_v,
     wq_v,
@@ -329,8 +331,6 @@
     kgain_v,
     hgain_v,
     wo_v,
-    kc_v,
-    vc_v,
     gc_v,
     send_q,
     send_kv,
@@ -341,6 +341,8 @@
     all_kv,
     send_part,
     got_part,
+    send_stats,
+    got_stats,
     all_normed,
     term_own,
     term_other,
@@ -359,14 +361,14 @@
     scale = head_size ** (-0.5)
     order = sorted(range(1, n), key=lambda step: abs(2 * step - n))
 
-    forget_rows = pl.ds(pl.multiple_of(me * width_in, width_in), width_in)
+    forget_columns = pl.ds(pl.multiple_of(me * width_in, width_in), width_in)
     loads = {}
     for index, (name, source, target) in enumerate(
         (
             ("tokens", tokens, tok_v),
             ("norm", norm_gain, norm_v),
             ("wq", w_query, wq_v),
-            ("wf", w_forget.at[forget_rows], wf_v),
+            ("wf", w_forget.at[:, forget_columns], wf_v),
             ("bias", forget_bias, bias_v),
             ("qgain", query_gain, qgain_v),
             ("kgain", key_gain, kgain_v),
@@ -425,7 +427,9 @@
     send_q[:, :, :head_width] = jnp.dot(
         scaled, wq_v[...], preferred_element_type=jnp.float32
     ).reshape(seqs, props, head_width)
-    gate_part = jnp.dot(scaled, wf_v[...], preferred_element_type=jnp.float32)
+    gate_part = lax.dot_general(
+        scaled, wf_v[...], (((1,), (1,)), ((), ())), preferred_element_type=jnp.float32
+    )
     gate_heads = gate_part.shape[1]
     send_q[:, :, head_width:] = jnp.broadcast_to(squares, (rows_all, LANES)).reshape(
         seqs, props, LANES
@@ -483,8 +487,17 @@
     logits = small[:, :gate_heads] * inverse + bias_v[...]
     logs = -(jnp.maximum(-logits, 0.0) + jnp.log1p(jnp.exp(-jnp.abs(logits))))
     logs = jnp.where(core == 0, logs[:, :heads], logs[:, heads:])
-    all_gates[me] = jnp.zeros((props, LANES), jnp.float32)
-    all_gates[me, :, :heads] = logs
+    side_row = lax.broadcasted_iota(jnp.int32, (props, LANES), 0)
+    side_column = lax.broadcasted_iota(jnp.int32, (props, LANES), 1)
+    turned = side_row == side_column
+    all_gates[me] = jnp.concatenate(
+        [
+            jnp.sum(jnp.where(turned, logs[:, head : head + 1], 0.0), axis=0, keepdims=True)
+            for head in range(heads)
+        ],
+        axis=0,
+    )
+    log_wide = pack_stats([logs[:, head : head + 1] for head in range(heads)], props)
     for step in order:
         push(2, step, lambda peer: send_kv.at[peer], got_kv)
     for step in order:
@@ -517,10 +530,13 @@
             )
             for head in range(heads)
         ]
-        send_part[seq, :, :head_width] = total
-        send_part[seq, :, head_width:] = pack_stats(peaks + totals + edges, props)
+        send_part[seq] = total.astype(jnp.bfloat16)
+        send_stats[seq] = pack_stats(peaks + totals + edges, props)
         if step:
             push(4, step, lambda peer: send_part.at[peer], got_part)
+            push(7, step, lambda peer: send_stats.at[peer], got_stats)
+        else:
+            own_total = total
 
     for step in order:
         arrive(2, step, got_kv)
@@ -537,7 +553,7 @@
 
     padding = jnp.zeros((LANES - props, head_width), jnp.bfloat16)
     log_tile = jnp.concatenate(
-        [all_gates[me], jnp.zeros((LANES - props, LANES), jnp.float32)], axis=0
+        [log_wide, jnp.zeros((LANES - props, LANES), jnp.float32)], axis=0
     )
     path_sum = jnp.dot(ancestors, log_tile, precision=lax.Precision.HIGHEST)
     on_diagonal = row == column
@@ -557,11 +573,13 @@
 
     for step in order:
         arrive(4, step, got_part)
-    parts = [send_part[me]] + [got_part[lax.rem(me + step, n)] for step in range(1, n)]
-    edge = functools.reduce(jnp.add, [part[:, head_width:] for part in parts])
-    tops = [spread_heads(part[:, head_width:], 0, heads, head_size) for part in parts]
-    sums = [spread_heads(part[:, head_width:], heads, heads, head_size) for part in parts]
-    numbers = [part[:, :head_width] for part in parts]
+        arrive(7, step, got_stats)
+    peers = [lax.rem(me + step, n) for step in range(1, n)]
+    stats = [send_stats[me]] + [got_stats[peer] for peer in peers]
+    edge = functools.reduce(jnp.add, stats)
+    tops = [spread_heads(each, 0, heads, head_size) for each in stats]
+    sums = [spread_heads(each, heads, heads, head_size) for each in stats]
+    numbers = [own_total] + [got_part[peer].astype(jnp.float32) for peer in peers]
     tops.append(
         spread_heads(tree_stats, 0, heads, head_size)
         - spread_heads(edge, 2 * heads, heads, head_size)
@@ -596,7 +614,7 @@
         arrive(3, step, all_gates)
     for step in order:
         arrive(5, step, all_kv)
-    out_gates[...] = all_gates[:, :, :heads]
+    out_gates[...] = all_gates[:, :, :props]
     out_rows[...] = all_kv[...]
     pair.wait()
     joined = term_own[...].astype(jnp.float32) + term_other[...].astype(jnp.float32)
@@ -617,24 +635,23 @@
     new_keys,
     new_values,
     gates_out,
-    kc_v,
-    vc_v,
+    windows,
     in_sem,
     out_sem,
 ):
-    seqs, pos_dev, head_width = kc_v.shape
+    seqs, pos_dev, head_width = key_cache.shape
     props = rows_in.shape[1]
     window = 2 * props
     start = lax.axis_index("kv") * pos_dev
-    caches = ((key_cache, kc_v, new_keys), (value_cache, vc_v, new_values))
-    loads = [
+    caches = ((key_cache, new_keys), (value_cache, new_values))
+    bulk = [
         [
-            pltpu.make_async_copy(source.at[seq], held.at[seq], in_sem.at[side, seq])
-            for side, (source, held, _) in enumerate(caches)
+            pltpu.make_async_copy(held.at[seq], target.at[seq], in_sem.at[side, seq])
+            for side, (held, target) in enumerate(caches)
         ]
         for seq in range(seqs)
     ]
-    for pair in loads:
+    for pair in bulk:
         for copy in pair:
             copy.start()
     layer_out[...] = layer_in[...]
@@ -642,7 +659,7 @@
     slot = lax.broadcasted_iota(jnp.int32, (window, props), 0)
     prop = lax.broadcasted_iota(jnp.int32, (window, props), 1)
     line = lax.broadcasted_iota(jnp.int32, (window, head_width), 0)
-    stores = []
+    patches = []
     for seq in range(seqs):
         offset = lengths[seq] + accepted[seq] - start
         inside = jnp.clip(offset, 0, pos_dev - 1)
@@ -651,19 +668,24 @@
         placing = (slot + lower - offset == prop).astype(jnp.float32).astype(jnp.bfloat16)
         place = line + lower - offset
         hit = (place >= 0) & (place < props)
-        for side, (_, held, target) in enumerate(caches):
+        for side, (held, target) in enumerate(caches):
             fresh = jnp.dot(
                 placing,
                 rows_in[seq, :, side * head_width : (side + 1) * head_width],
                 preferred_element_type=jnp.float32,
             )
-            loads[seq][side].wait()
             kept = held[seq, rows, :].astype(jnp.float32)
-            held[seq, rows, :] = jnp.where(hit, fresh, kept).astype(jnp.bfloat16)
-            copy = pltpu.make_async_copy(held.at[seq], target.at[seq], out_sem.at[side, seq])
-            copy.start()
-            stores.append(copy)
-    for copy in stores:
+            windows[side, seq] = jnp.where(hit, fresh, kept).astype(jnp.bfloat16)
+            patches.append(
+                pltpu.make_async_copy(
+                    windows.at[side, seq], target.at[seq, rows, :], out_sem.at[side, seq]
+                )
+            )
+    for seq in range(seqs):
+        for side in range(2):
+            bulk[seq][side].wait()
+            patches[2 * seq + side].start()
+    for copy in patches:
         copy.wait()
 
 
@@ -695,7 +717,7 @@
     bf16, f32 = jnp.bfloat16, jnp.float32
     smem = pl.BlockSpec(memory_space=pltpu.SMEM)
     vmem = pl.BlockSpec(memory_space=pltpu.VMEM)
-    any_space = pl.BlockSpec(memory_space=pl.ANY)
+    any_space = pl.BlockSpec(memory_space=pltpu.HBM)
     line = lambda vector: vector.reshape(1, -1)
     operands = (
         tokens,
@@ -703,7 +725,7 @@
         w_query,
         w_key,
         w_value,
-        w_forget,
+        w_forget.T,
         line(forget_bias),
         line(query_gain),
         line(key_gain),
@@ -720,46 +742,50 @@
         pltpu.VMEM(w_query.shape, bf16),
         pltpu.VMEM(w_key.shape, bf16),
         pltpu.VMEM(w_value.shape, bf16),
-        pltpu.VMEM((width_in, w_forget.shape[1]), bf16),
+        pltpu.VMEM((w_forget.shape[1], width_in), bf16),
         pltpu.VMEM((1, forget_bias.shape[0]), f32),
         pltpu.VMEM((1, head_size), f32),
         pltpu.VMEM((1, head_size), f32),
         pltpu.VMEM((1, head_size), f32),
         pltpu.VMEM(w_out.shape, bf16),
-        pltpu.VMEM(key_cache.shape, bf16),
-        pltpu.VMEM(value_cache.shape, bf16),
         pltpu.VMEM(gate_cache.shape, f32),
         pltpu.VMEM((seqs, props, part_width), f32),
         pltpu.VMEM((seqs, props, 2 * head_width), f32),
         pltpu.VMEM((n, props, part_width), f32),
         pltpu.VMEM((n, props, 2 * head_width), f32),
         pltpu.VMEM((n, props, head_width), bf16),
+        pltpu.VMEM((n, heads, LANES), f32),
+        pltpu.VMEM((n, props, 2 * head_width), bf16),
+        pltpu.VMEM((seqs, props, head_width), bf16),
+        pltpu.VMEM((n, props, head_width), bf16),
+        pltpu.VMEM((seqs, props, LANES), f32),
         pltpu.VMEM((n, props, LANES), f32),
-        pltpu.VMEM((n, props, 2 * head_width), bf16),
-        pltpu.VMEM((seqs, props, part_width), f32),
-        pltpu.VMEM((n, props, part_width), f32),
         pltpu.VMEM((n, props, head_width), bf16),
         pltpu.VMEM((seqs * props, width_out), bf16),
         pltpu.VMEM((seqs * props, width_out), bf16),
         pltpu.SemaphoreType.DMA((14,)),
-        pltpu.SemaphoreType.DMA((7, n)),
-        pltpu.SemaphoreType.DMA((7, n)),
+        pltpu.SemaphoreType.DMA((8, n)),
+        pltpu.SemaphoreType.DMA((8, n)),
         pltpu.SemaphoreType.DMA((2,)),
     ]
-    layer, rows, gates = pl.pallas_call(
+    layer, rows, gates, *held = pl.pallas_call(
         functools.partial(layer_kernel, (n, heads, head_size, w_forget.shape[0])),
         out_shape=(
-            jax.ShapeDtypeStruct((seqs, props, width_out), bf16),
-            jax.ShapeDtypeStruct((seqs, props, 2 * head_width), bf16),
-            jax.ShapeDtypeStruct((seqs, props, heads), f32),
+            pltpu.VMEM((seqs, props, width_out), bf16),
+            pltpu.VMEM((seqs, props, 2 * head_width), bf16),
+            pltpu.VMEM((seqs, heads, props), f32),
+            pltpu.VMEM(key_cache.shape, bf16),
+            pltpu.VMEM(value_cache.shape, bf16),
         ),
         in_specs=[smem] * 3 + [any_space] * len(operands),
-        out_specs=(vmem, vmem, vmem),
+        out_specs=(vmem,) * 5,
         scratch_shapes=scratch,
-        compiler_params=pltpu.CompilerParams(collective_id=0, has_side_effects=True),
+        compiler_params=pltpu.CompilerParams(
+            collective_id=0, has_side_effects=True, vmem_limit_bytes=62586880
+        ),
         name="layer",
     )(lengths, accepted, parents, *operands)
-    return pl.pallas_call(
+    layer, new_keys, new_values, gates = pl.pallas_call(
         write_kernel,
         out_shape=(
             jax.ShapeDtypeStruct(layer.shape, bf16),
@@ -767,16 +793,17 @@
             jax.ShapeDtypeStruct(value_cache.shape, bf16),
             jax.ShapeDtypeStruct(gates.shape, f32),
         ),
-        in_specs=[smem, smem, vmem, vmem, vmem, any_space, any_space],
+        in_specs=[smem, smem] + [vmem] * 5,
         out_specs=(vmem, any_space, any_space, vmem),
         scratch_shapes=[
-            pltpu.VMEM(key_cache.shape, bf16),
-            pltpu.VMEM(value_cache.shape, bf16),
+            pltpu.VMEM((2, seqs, 2 * props, head_width), bf16),
             pltpu.SemaphoreType.DMA((2, seqs)),
             pltpu.SemaphoreType.DMA((2, seqs)),
         ],
+        compiler_params=pltpu.CompilerParams(vmem_limit_bytes=16 << 20),
         name="write",
-    )(lengths, accepted, layer, rows, gates, key_cache, value_cache)
+    )(lengths, accepted, layer, rows, gates, *held)
+    return layer, new_keys, new_values, jnp.swapaxes(gates, 1, 2)
 
 
 def pick_shards(n, cores):

time: 39.9 us -> 33.1 us (0.83)
  Pallas kernels: 35.7 us -> 32.2 us
  local copies, waits for them, and re-layouts: 3.28 us -> 0.01 us
    pallas_call x1, Pallas kernels: 30.5 us -> 28.3 us  [fused_shards(): pl.pallas_call(functools.partial(layer_kernel, (n, heads, head_size, w_fo...]
    unnamed x1 -> x4, local copies, waits for them, and re-layouts: 1.84 us -> 0.01 us
    pallas_call x1 -> x0, local copies, waits for them, and re-layouts: 1.44 us -> none  [fused_shards(): pl.pallas_call(write_kernel, out_shape=(jax.ShapeDtypeStruct(layer.shape,...]
    pallas_call x1, Pallas kernels: 5.12 us -> 3.96 us  [fused_shards(): pl.pallas_call(write_kernel, out_shape=(jax.ShapeDtypeStruct(layer.shape,...]
where the time goes in v2:
time: 33.1 us; the launch traced here: 32.9 us
  Pallas kernels  32.2 us (97%)
  between operations  0.68 us (2%)
    pallas_call x1, Pallas kernels, fused_shards(): pl.pallas_call(functools.partial(layer_kernel, (n, heads, head_size, w_fo...  28.3 us
    pallas_call x1, Pallas kernels, fused_shards(): pl.pallas_call(write_kernel, out_shape=(jax.ShapeDtypeStruct(layer.shape,...  3.96 us

profile of v2, /device:TPU:0, one launch (start us, length us, event | category | flops | bytes accessed | tf_op | source)
XLA Modules:
  0.0 32.9 jit_solution(8617854773773363308)
XLA Ops:
  0.6 0.0 copy-start
  0.6 0.0 copy-start.1
  0.7 28.3 %layer.1 = (bf16[4,16,512]{2,1,0:T(8,128)(2,1)S(1)}, bf16[4,16,1024]{2,1,0:T(8,128)(2,1)S(1)}, f32[4,8,16]{2,1,0:T(8,128)S(1)}, bf16[4,512,512]{2,1,0:T(8,128)(2,1)S(1)}, bf16[4,512,512]{2,1,0:T(8,128)(2,1)S(1)}) custom-call(s32[4]{0:T(128)} %lengths.3, s32[4]{0:T(128)} %accepted.3, s32[4,16]{1,0:T(4,128)} %parents.1, bf16[4,16,512]{2,1,0:T(8,128)(2,1)} %tokens.1, ...), custom_call_target="tpu_custom_call" | custom-call | tf_op jit(solution)/shard_map/layer/pallas_call | solution.py:771
  28.9 0.0 copy-done
  29.0 0.0 copy-done.1
  29.0 4.0 %write.1 = (bf16[4,16,512]{2,1,0:T(8,128)(2,1)}, bf16[4,512,512]{2,1,0:T(8,128)(2,1)}, bf16[4,512,512]{2,1,0:T(8,128)(2,1)}, f32[4,8,16]{2,1,0:T(8,128)}) custom-call(s32[4]{0:T(128)S(1)} %copy-done, s32[4]{0:T(128)S(1)} %copy-done.1, bf16[4,16,512]{2,1,0:T(8,128)(2,1)S(1)} %get-tuple-element.13.layer_in, ...), custom_call_target="tpu_custom_call" | custom-call | tf_op jit(solution)/shard_map/write/pallas_call | solution.py:788
Async XLA Ops:
  0.6 28.3 %copy-start = (s32[4]{0:T(128)S(1)}, s32[4]{0:T(128)}, u32[]{:S(2)}) copy-start(s32[4]{0:T(128)} %lengths.3) | copy-start | bytes 52
  0.6 28.3 %copy-start.1 = (s32[4]{0:T(128)S(1)}, s32[4]{0:T(128)}, u32[]{:S(2)}) copy-start(s32[4]{0:T(128)} %accepted.3) | copy-start | bytes 52
